TPU v7x, 32 devices: a whole 2x2x4 slice. The times are simulated.
32 devices in a mesh: fs: 8 (over z, x), tp: 4 (over y, core).
Axes of the slice: x: 2, y: 2, z: 4, core: 2. Of those that a mesh axis runs over, the one named last changes fastest.
Arguments:
- seq_rows: bfloat16 [6144, 2048], P('fs', 'tp'), may hold values from -6 to 6
- mixer_gain: bfloat16 [2048], P('tp'), may hold values from 0.099609375 to 1.8984375
- query_weight: bfloat16 [2048, 2048], P('fs', 'tp'), may hold values from -0.125 to 0.125
- key_weight: bfloat16 [2048, 2048], P('fs', 'tp'), may hold values from -0.125 to 0.125
- value_weight: bfloat16 [2048, 4096], P('fs', 'tp'), may hold values from -0.125 to 0.125
- decay_logs: float32 [8], P('tp'), may hold values from -0.0333333333 to -0.000390625
- mixer_out_weight: bfloat16 [4096, 2048], P('tp', 'fs'), may hold values from -0.125 to 0.125
- channel_gain: bfloat16 [2048], P('tp'), may hold values from 0.099609375 to 1.8984375
- value_up_weight: bfloat16 [2048, 5632], P('fs', 'tp'), may hold values from -0.125 to 0.125
- gate_up_weight: bfloat16 [2048, 5632], P('fs', 'tp'), may hold values from -0.125 to 0.125
- conv_taps: bfloat16 [3, 5632], P(None, 'tp'), may hold values from -3 to 3
- conv_bias: bfloat16 [5632], P('tp'), may hold values from -3 to 3
- down_weight: bfloat16 [5632, 2048], P('tp', 'fs'), may hold values from -0.109375 to 0.109375
Outputs:
- layer_out: bfloat16 [6144, 2048], P('fs', 'tp')
All inputs are finite; a program needn't handle non-finite values.
Results may differ from a plain program's by a relative error of at most 0.02.
Values may be sent and summed in bfloat16 or wider, within the bound.
A program may use at most 128 MiB of HBM per device.

v0:
```python
import jax
import jax.numpy as jnp
from jax import lax
from jax.sharding import PartitionSpec as P

DK = 256
DV = 512
KW = 3
BLOCK = 128
EPS = 1e-06
ROPE_BASE = 10000.0
HIGH_PRECISION = lax.Precision.HIGHEST


def rotate_heads(tensor, cosine, sine):
    half = tensor.shape[-1] // 2
    first = tensor[..., :half]
    second = tensor[..., half:]
    return jnp.concatenate(
        [first * cosine - second * sine, first * sine + second * cosine], axis=-1
    )


def retention_blocks(query, key, value, decay_logs):
    length, heads = (query.shape[0], query.shape[1])
    count = length // BLOCK
    offsets = jnp.arange(BLOCK, dtype=jnp.float32)
    spread = offsets[:, None] - offsets[None, :]
    within_block = jnp.where(
        spread[None] >= 0.0,
        jnp.exp(decay_logs[:, None, None] * jnp.maximum(spread, 0.0)[None]),
        0.0,
    )
    carried = jnp.exp(decay_logs[:, None] * (offsets + 1.0))
    state_decay_factor = jnp.exp(decay_logs[:, None] * (BLOCK - 1.0 - offsets))
    block_decay_factor = jnp.exp(decay_logs * BLOCK)

    def blocks(tensor):
        return tensor.reshape(count, BLOCK, heads, tensor.shape[-1]).transpose(0, 2, 1, 3)

    def advance(recurrent_state, triple):
        query_block, key_block, value_block = triple
        attention_scores = (
            jnp.einsum("ucf,uxf->ucx", query_block, key_block, precision=HIGH_PRECISION)
            * within_block
        )
        result = jnp.einsum("hnm,hmv->hnv", attention_scores, value_block, precision=HIGH_PRECISION)
        result = (
            result
            + jnp.einsum("hnd,hdv->hnv", query_block, recurrent_state, precision=HIGH_PRECISION)
            * carried[:, :, None]
        )
        recurrent_state = block_decay_factor[:, None, None] * recurrent_state + jnp.einsum(
            "ieb,iez->ibz",
            key_block * state_decay_factor[:, :, None],
            value_block,
            precision=HIGH_PRECISION,
        )
        return (recurrent_state, result)

    start = jnp.zeros((heads, query.shape[-1], value.shape[-1]), jnp.float32)
    _, result = lax.scan(advance, start, (blocks(query), blocks(key), blocks(value)))
    return result.transpose(0, 2, 1, 3).reshape(length, heads, value.shape[-1])


def normalise(whole_rows, gain_row):
    rows_f = whole_rows.astype(jnp.float32)
    factor = lax.rsqrt(jnp.mean(rows_f * rows_f, axis=-1, keepdims=True) + EPS)
    scaled = (rows_f * gain_row.astype(jnp.float32)[None, :]).astype(jnp.bfloat16)
    return (factor, scaled)


def on_device(
    seq_rows,
    mixer_gain,
    query_weight,
    key_weight,
    value_weight,
    decay_logs,
    mixer_out_weight,
    channel_gain,
    value_up_weight,
    gate_up_weight,
    conv_taps,
    conv_bias,
    down_weight,
):
    length = seq_rows.shape[0]
    hidden_part = value_up_weight.shape[1]
    heads_here = query_weight.shape[1] // DK
    whole_rows, gains = (
        lax.all_gather(seq_rows, "tp", axis=1, tiled=True),
        lax.all_gather(jnp.stack([mixer_gain, channel_gain]), "tp", axis=1, tiled=True),
    )
    factor_one, scaled_one = normalise(whole_rows, gains[0])
    pieces = (
        lax.all_gather(query_weight, "fs", axis=0, tiled=True),
        lax.all_gather(key_weight, "fs", axis=0, tiled=True),
        lax.all_gather(value_weight, "fs", axis=0, tiled=True),
    )
    columns = scaled_one
    sum_q, sum_k, sum_v = tuple(
        (jnp.dot(columns, piece, preferred_element_type=jnp.float32) for piece in pieces)
    )
    query = (sum_q * factor_one).astype(jnp.bfloat16)
    key = (sum_k * factor_one).astype(jnp.bfloat16)
    value = (sum_v * factor_one).astype(jnp.bfloat16)
    half = DK // 2
    freqs = jnp.power(ROPE_BASE, -jnp.arange(half, dtype=jnp.float32) * 2.0 / DK)
    angles = jnp.arange(length, dtype=jnp.float32)[:, None] * freqs[None, :]
    cosine = jnp.cos(angles)[:, None, :]
    sine = jnp.sin(angles)[:, None, :]
    turned_q = rotate_heads(query.astype(jnp.float32).reshape(length, heads_here, DK), cosine, sine)
    turned_k = rotate_heads(
        key.astype(jnp.float32).reshape(length, heads_here, DK), cosine, sine
    ) * DK ** (-0.5)
    ret = retention_blocks(
        turned_q, turned_k, value.astype(jnp.float32).reshape(length, heads_here, DV), decay_logs
    )
    centred = ret - jnp.mean(ret, axis=-1, keepdims=True)
    normed = (
        (centred * lax.rsqrt(jnp.mean(centred * centred, axis=-1, keepdims=True) + EPS))
        .reshape(length, heads_here * DV)
        .astype(jnp.bfloat16)
    )
    mixed_terms = jnp.dot(
        normed,
        lax.all_gather(mixer_out_weight, "fs", axis=1, tiled=True),
        preferred_element_type=jnp.float32,
    )
    mixed = lax.psum_scatter(
        mixed_terms.astype(jnp.bfloat16), "tp", scatter_dimension=1, tiled=True
    ).astype(jnp.float32)
    middle = (seq_rows.astype(jnp.float32) + mixed).astype(jnp.bfloat16)
    middle_whole = lax.all_gather(middle, "tp", axis=1, tiled=True)
    factor_two, scaled_two = normalise(middle_whole, gains[1])
    pieces = (
        lax.all_gather(value_up_weight, "fs", axis=0, tiled=True),
        lax.all_gather(gate_up_weight, "fs", axis=0, tiled=True),
    )
    columns = scaled_two
    sum_val = jnp.dot(columns, pieces[0], preferred_element_type=jnp.float32)
    sum_gate = jnp.dot(columns, pieces[1], preferred_element_type=jnp.float32)
    up_val = (sum_val * factor_two).astype(jnp.bfloat16)
    up_gate = (sum_gate * factor_two).astype(jnp.bfloat16)
    padded = jnp.concatenate(
        [jnp.zeros((KW - 1, hidden_part), jnp.float32), up_gate.astype(jnp.float32)], axis=0
    )
    conv = jnp.zeros((length, hidden_part), jnp.float32) + conv_bias.astype(jnp.float32)[None, :]
    for tap in range(KW):
        conv = conv + conv_taps[tap].astype(jnp.float32)[None, :] * padded[tap : tap + length]
    hidden = (jax.nn.silu(conv) * up_val.astype(jnp.float32)).astype(jnp.bfloat16)
    channel_terms = jnp.dot(
        hidden,
        lax.all_gather(down_weight, "fs", axis=1, tiled=True),
        preferred_element_type=jnp.float32,
    )
    channel = lax.psum_scatter(
        channel_terms.astype(jnp.bfloat16), "tp", scatter_dimension=1, tiled=True
    ).astype(jnp.float32)
    return (middle.astype(jnp.float32) + channel).astype(jnp.bfloat16)


def solution(mesh):
    placed = (
        P("fs", "tp"),
        P("tp"),
        P("fs", "tp"),
        P("fs", "tp"),
        P("fs", "tp"),
        P("tp"),
        P("tp", "fs"),
        P("tp"),
        P("fs", "tp"),
        P("fs", "tp"),
        P(None, "tp"),
        P("tp"),
        P("tp", "fs"),
    )
    return jax.shard_map(
        on_device, mesh=mesh, in_specs=placed, out_specs=P("fs", "tp"), check_vma=False
    )
```

profile of v0, /device:TPU:0, one launch (start us, length us, event | category | flops | bytes accessed | tf_op | source)
XLA Modules:
  0.0 714.1 jit_solution(16851320233970541097)
XLA Ops:
  6.5 0.7 all-gather.10.cloned.1.call-update
  7.3 0.7 all-gather.12.cloned.1.call-update
  11.5 6.2 all_gather.31
  18.3 2.2 fusion.56
  20.5 19.6 %all-gather.10.cloned.1.call-done = bf16[768,2048]{1,0:T(8,128)(2,1)} async-done(((bf16[768,512]{1,0:T(8,128)(2,1)}), bf16[768,2048]{1,0:T(8,128)(2,1)}) %all-gather.10.cloned.1.call-update) | async-done | bytes 3145744 | tf_op jit(solution)/shard_map/all_gather | solution.py:92
  40.2 2.6 fusion.31
  42.7 48.7 %all-gather.12.cloned.1.call-done = bf16[2048,512]{1,0:T(8,128)(2,1)} async-done(((bf16[256,512]{1,0:T(8,128)(2,1)}), bf16[2048,512]{1,0:T(8,128)(2,1)}) %all-gather.12.cloned.1.call-update) | async-done | bytes 2097168 | tf_op jit(solution)/shard_map/all_gather | solution.py:98
  91.4 4.4 multiply_convert_fusion.7
  96.5 44.7 %all-gather.16.cloned.1.call-done = bf16[2048,512]{1,0:T(8,128)(2,1)} async-done(((bf16[256,512]{1,0:T(8,128)(2,1)}), bf16[2048,512]{1,0:T(8,128)(2,1)}) %all-gather.16.cloned.1.call-update) | async-done | bytes 2097168 | tf_op jit(solution)/shard_map/all_gather | solution.py:97
  141.2 4.4 multiply_convert_fusion.6
  145.6 1.3 fusion.62
  146.9 1.4 copy.42
  148.3 2.3 copy.43
  150.6 1.7 multiply_subtract_fusion
  152.4 1.3 fusion.48
  153.7 60.8 %all-gather.14.cloned.1.call-done = bf16[2048,1024]{1,0:T(8,128)(2,1)} async-done(((bf16[256,1024]{1,0:T(8,128)(2,1)}), bf16[2048,1024]{1,0:T(8,128)(2,1)}) %all-gather.14.cloned.1.call-update) | async-done | bytes 4194320 | tf_op jit(solution)/shard_map/all_gather | solution.py:99
  214.5 8.2 %fusion.45 = f32[768,1024]{1,0:T(8,128)} fusion(bf16[2048,1024]{1,0:T(8,128)(2,1)} %all-gather.14.cloned.1.call-done, bf16[768,2048]{1,0:T(8,128)(2,1)} %all-gather.10.cloned.1.call-done, f32[2048]{0:T(1024)S(1)} %bitcast.94, f32[768]{0:T(1024)S(1)} %add_rsqrt_fusion.1), kind=kOutput, calls=%fused_computation.54 | convolution fusion | flops 3228303360 | bytes 10497024 | tf_op jit(solution)/shard_map/dot_general | solution.py:103
  222.7 5.6 reshape.163
  228.3 4.1 copy.48
  232.5 42.6 %while.15 = (s32[]{:T(128)}, f32[2,256,512]{2,1,0:T(8,128)S(1)}, f32[6,2,128,512]{3,2,1,0:T(8,128)}, f32[2]{0:T(128)S(1)}, f32[6,2,128,256]{3,2,0,1:T(8,128)}, /...) while((s32[]{:T(128)}, f32[2,256,512]{2,1,0:T(8,128)S(1)}, ...), condition=%wide.region_2.3_spmd.clone.clone.clone, body=%wide.region_1.2_spmd.clone.clone.clone.sunk | while | flops 1108771328 | bytes 7169184 | solution.py:62
  232.5 1.3 convolution_multiply_fusion.3
  233.8 1.6 fusion.88
  235.6 1.6 fusion.89
  237.2 2.5 convolution_add_fusion.2
  239.6 1.4 convolution_multiply_fusion.3
  241.0 1.6 fusion.88
  242.7 1.5 fusion.89
  244.2 2.5 convolution_add_fusion.2
  246.7 1.4 convolution_multiply_fusion.3
  248.1 1.6 fusion.88
  249.8 1.5 fusion.89
  251.3 2.5 convolution_add_fusion.2
  253.8 1.4 convolution_multiply_fusion.3
  255.2 1.6 fusion.88
  256.9 1.6 fusion.89
  258.5 2.5 convolution_add_fusion.2
  260.9 1.4 convolution_multiply_fusion.3
  262.3 1.6 fusion.88
  264.0 1.5 fusion.89
  265.6 2.5 convolution_add_fusion.2
  268.0 1.4 convolution_multiply_fusion.3
  269.4 1.6 fusion.88
  271.1 1.5 fusion.89
  272.6 2.5 convolution_add_fusion.2
  275.1 2.4 bitcast_reduce_fusion
  278.8 1.1 mul.367
  279.9 2.5 copy.46
  282.6 1.1 sub.65
  283.6 2.5 copy.45
  286.1 2.4 copy.34
  288.6 2.4 copy.44
  291.0 9.3 %convolution_convert_fusion = bf16[768,2048]{1,0:T(8,128)(2,1)} fusion(bf16[1024,2048]{1,0:T(8,128)(2,1)} %all-gather.18.cloned.1.call-done, f32[768,1024]{1,0:T(8,128)S(1)} %bitcast.83, f32[768,1024]{1,0:T(8,128)} %bitcast.85, f32[768,1024]{1,0:T(8,128)} %bitcast.84), kind=kOutput, calls=%fused_computation.44 | convolution fusion | flops 3225157632 | bytes 16777216 | tf_op jit(solution)/shard_map/dot_general | solution.py:126
  300.3 36.5 %reduce-scatter.3.cloned.1.call-done = bf16[768,512]{1,0:T(8,128)(2,1)} async-done(((bf16[768,2048]{1,0:T(8,128)(2,1)}), bf16[768,512]{1,0:T(8,128)(2,1)}) %reduce-scatter.3.cloned.1.call-update) | async-done | bytes 786448 | tf_op jit(solution)/shard_map/reduce_scatter | solution.py:131
  336.8 2.2 add_convert_fusion.1
  339.1 0.7 all-gather.22.cloned.1.call-update
  341.3 26.5 %all-gather.20.cloned.1.call-done = bf16[768,2048]{1,0:T(8,128)(2,1)} async-done(((bf16[768,512]{1,0:T(8,128)(2,1)}), bf16[768,2048]{1,0:T(8,128)(2,1)}) %all-gather.20.cloned.1.call-update) | async-done | bytes 3145744 | tf_op jit(solution)/shard_map/all_gather | solution.py:135
  367.7 2.7 fusion.33
  370.5 91.8 %all-gather.22.cloned.1.call-done = bf16[2048,1408]{1,0:T(8,128)(2,1)} async-done(((bf16[256,1408]{1,0:T(8,128)(2,1)}), bf16[2048,1408]{1,0:T(8,128)(2,1)}) %all-gather.22.cloned.1.call-update) | async-done | bytes 5767184 | tf_op jit(solution)/shard_map/all_gather | solution.py:139
  462.2 9.2 %fusion.34 = f32[768,1408]{1,0:T(8,128)} fusion(bf16[2048,1408]{1,0:T(8,128)(2,1)} %all-gather.22.cloned.1.call-done, bf16[768,2048]{1,0:T(8,128)(2,1)S(1)} %copy-done.2, f32[2048]{0:T(1024)S(1)} %bitcast.90, f32[768]{0:T(1024)S(1)} %add_rsqrt_fusion), kind=kOutput, calls=%fused_computation.45 | convolution fusion | flops 4437147648 | bytes 13249536 | tf_op jit(solution)/shard_map/dot_general | solution.py:143
  471.5 83.5 %all-gather.24.cloned.1.call-done = bf16[2048,1408]{1,0:T(8,128)(2,1)} async-done(((bf16[256,1408]{1,0:T(8,128)(2,1)}), bf16[2048,1408]{1,0:T(8,128)(2,1)}) %all-gather.24.cloned.1.call-update) | async-done | bytes 5767184 | tf_op jit(solution)/shard_map/all_gather | solution.py:138
  555.0 93.2 %all-gather.26.cloned.1.call-done = bf16[1408,2048]{1,0:T(8,128)(2,1)} async-done(((bf16[1408,256]{1,0:T(8,128)(2,1)}), bf16[1408,2048]{1,0:T(8,128)(2,1)}) %all-gather.26.cloned.1.call-update) | async-done | bytes 5767184 | tf_op jit(solution)/shard_map/all_gather | solution.py:155
  648.2 21.1 %convolution_convert_fusion.1 = bf16[768,2048]{1,0:T(8,128)(2,1)} fusion(bf16[1408,2048]{1,0:T(8,128)(2,1)} %all-gather.26.cloned.1.call-done, f32[768,1408]{1,0:T(8,128)} %fusion.34, bf16[2048,1408]{1,0:T(8,128)(2,1)} %all-gather.24.cloned.1.call-done, bf16[768,2048]{1,0:T(8,128)(2,1)S(1)} %copy-done.2, f32[2048]{0:T(1024)S(1)} %bitcast.91, ...), kind=kOutput, calls=%fused_computation.46 | convolution fusion | flops 8880881664 | bytes 22184960 | tf_op jit(solution)/shard_map/dot_general | solution.py:153
  669.3 36.1 %reduce-scatter.5.cloned.1.call-done = bf16[768,512]{1,0:T(8,128)(2,1)} async-done(((bf16[768,2048]{1,0:T(8,128)(2,1)}), bf16[768,512]{1,0:T(8,128)(2,1)}) %reduce-scatter.5.cloned.1.call-update) | async-done | bytes 786448 | tf_op jit(solution)/shard_map/reduce_scatter | solution.py:158
  705.4 2.2 add_convert_fusion
  (68 shorter events, 8.3 us)
Async XLA Ops:
  6.5 14.0 %copy-start.5 = (f32[2]{0:T(128)S(1)}, f32[2]{0:T(128)}, u32[]{:S(2)}) copy-start(f32[2]{0:T(128)} %param.20) | copy-start | bytes 28
  6.5 33.6 %all-gather.10.cloned.1.call-start = ((), (), s32[]{:S(2)}) async-start(), calls=%async_computation.2 | async-start | bytes 3932160 | tf_op jit(solution)/shard_map/all_gather | solution.py:92
  7.3 84.1 %all-gather.12.cloned.1.call-start = ((), (), s32[]{:S(2)}) async-start(), calls=%async_computation.3 | async-start | bytes 2359296 | tf_op jit(solution)/shard_map/all_gather | solution.py:98
  8.0 133.2 %all-gather.16.cloned.1.call-start = ((), (), s32[]{:S(2)}) async-start(), calls=%async_computation.5 | async-start | bytes 2359296 | tf_op jit(solution)/shard_map/all_gather | solution.py:97
  8.7 205.8 %all-gather.14.cloned.1.call-start = ((), (), s32[]{:S(2)}) async-start(), calls=%async_computation.4 | async-start | bytes 4718592 | tf_op jit(solution)/shard_map/all_gather | solution.py:99
  9.3 281.7 %all-gather.18.cloned.1.call-start = ((), (), s32[]{:S(2)}) async-start(), calls=%async_computation.6 | async-start | bytes 4718592 | tf_op jit(solution)/shard_map/all_gather | solution.py:128
  9.9 326.9 %reduce-scatter.3.cloned.1.call-start = ((), (), s32[]{:S(2)}) async-start(), calls=%async_computation.7 | async-start | bytes 3932160 | tf_op jit(solution)/shard_map/reduce_scatter | solution.py:131
  275.1 2.9 copy-start
  288.5 2.4 copy-start.3
  300.2 36.6 %copy-start.4 = (bf16[768,512]{1,0:T(8,128)(2,1)S(1)}, bf16[768,512]{1,0:T(8,128)(2,1)}, u32[]{:S(2)}) copy-start(bf16[768,512]{1,0:T(8,128)(2,1)} %param.15) | copy-start | bytes 2359300
  300.3 40.9 %copy-start.8 = (bf16[1408]{0:T(1024)(128)(2,1)S(1)}, bf16[1408]{0:T(1024)(128)(2,1)}, u32[]{:S(2)}) copy-start(bf16[1408]{0:T(1024)(128)(2,1)} %param.26) | copy-start | bytes 8452
  300.3 40.9 %copy-start.6 = (bf16[3,1408]{1,0:T(4,128)(2,1)S(1)}, bf16[3,1408]{1,0:T(4,128)(2,1)}, u32[]{:S(2)}) copy-start(bf16[3,1408]{1,0:T(4,128)(2,1)} %param.25) | copy-start | bytes 25348
  300.3 67.4 %all-gather.20.cloned.1.call-start = ((), (), s32[]{:S(2)}) async-start(), calls=%async_computation.8 | async-start | bytes 3932160 | tf_op jit(solution)/shard_map/all_gather | solution.py:135
  339.0 123.2 %copy-start.7 = (f32[1,2048]{1,0:T(1,128)S(1)}, f32[1,2048]{1,0:T(1,128)}, u32[]{:S(2)}) copy-start(f32[1,2048]{1,0:T(1,128)} %get-tuple-element.238) | copy-start | bytes 24580
  339.0 123.2 %all-gather.22.cloned.1.call-start = ((), (), s32[]{:S(2)}) async-start(), calls=%async_computation.9 | async-start | bytes 6488064 | tf_op jit(solution)/shard_map/all_gather | solution.py:139
  339.8 215.2 %all-gather.24.cloned.1.call-start = ((), (), s32[]{:S(2)}) async-start(), calls=%async_computation.10 | async-start | bytes 6488064 | tf_op jit(solution)/shard_map/all_gather | solution.py:138
  340.5 307.7 %all-gather.26.cloned.1.call-start = ((), (), s32[]{:S(2)}) async-start(), calls=%async_computation.11 | async-start | bytes 6488064 | tf_op jit(solution)/shard_map/all_gather | solution.py:155
  341.1 364.3 %reduce-scatter.5.cloned.1.call-start = ((), (), s32[]{:S(2)}) async-start(), calls=%async_computation.12 | async-start | bytes 3932160 | tf_op jit(solution)/shard_map/reduce_scatter | solution.py:158
  367.7 94.5 %copy-start.2 = (bf16[768,2048]{1,0:T(8,128)(2,1)S(1)}, bf16[768,2048]{1,0:T(8,128)(2,1)}, u32[]{:S(2)}) copy-start(bf16[768,2048]{1,0:T(8,128)(2,1)} %all-gather.20.cloned.1.call-done) | copy-start | bytes 9437188
  669.3 36.1 %copy-start.1 = (bf16[768,512]{1,0:T(8,128)(2,1)S(1)}, bf16[768,512]{1,0:T(8,128)(2,1)}, u32[]{:S(2)}) copy-start(bf16[768,512]{1,0:T(8,128)(2,1)} %add_convert_fusion.1) | copy-start | bytes 2359300
Sparse Core Ops, SparseCore 0:
  8.9 31.2 all-gather.9
  42.3 49.0 all-gather.11
  93.5 47.6 all-gather.15
  143.2 71.3 all-gather.13
  216.4 73.1 all-gather.17
  300.4 36.3 reduce-scatter.2
  339.2 28.5 all-gather.19
  369.9 92.2 all-gather.21
  464.4 90.4 all-gather.23
  556.8 91.2 all-gather.25
  669.4 35.9 reduce-scatter.4
where the time goes:
time: 715 us; the launch traced here: 714 us
  waiting for transfers between devices  546 us (76%)
  matrix products  98.5 us (14%)
  local copies, waits for them, and re-layouts  29.7 us (4%)
  other arithmetic  19.2 us (3%)
  between operations  13.5 us (2%)
    all_gather x1, waiting for transfers between devices, on_device(): lax.all_gather(down_weight, 'fs', axis=1, tiled=True)  93.2 us
    all_gather x1, waiting for transfers between devices, on_device(): lax.all_gather(gate_up_weight, 'fs', axis=0, tiled=True)  91.8 us
    all_gather x1, waiting for transfers between devices, on_device(): lax.all_gather(value_up_weight, 'fs', axis=0, tiled=True)  83.5 us
    all_gather x1, waiting for transfers between devices, on_device(): lax.all_gather(value_weight, 'fs', axis=0, tiled=True)  60.8 us
    all_gather x1, waiting for transfers between devices, on_device(): lax.all_gather(key_weight, 'fs', axis=0, tiled=True)  48.7 us
    all_gather x1, waiting for transfers between devices, on_device(): lax.all_gather(query_weight, 'fs', axis=0, tiled=True)  44.7 us
    reduce_scatter x1, waiting for transfers between devices, on_device(): lax.psum_scatter(mixed_terms.astype(jnp.bfloat16), 'tp', scatter_dimensio...  36.5 us
    reduce_scatter x1, waiting for transfers between devices, on_device(): lax.psum_scatter(channel_terms.astype(jnp.bfloat16), 'tp', scatter_dimens...  36.1 us
  transfers between devices with their start and end apart: 11, of which 10 were waited for; matrix products, arithmetic and copies ran while one was open for 16% of the time, Pallas kernels for 0%

commit v1 on v0

--- a/solution.py
+++ b/solution.py
@@ -10,6 +10,12 @@
 EPS = 1e-06
 ROPE_BASE = 10000.0
 HIGH_PRECISION = lax.Precision.HIGHEST
+
+
+def keep_up_ranges(w_in):
+    return jnp.concatenate(
+        lax.all_to_all(jnp.stack([w_in for _ in range(lax.psum(1, "fs"))], 0), "fs", 0, 0), 0
+    )
 
 
 def rotate_heads(tensor, cosine, sine):
@@ -95,7 +101,7 @@
     factor_one, scaled_one = normalise(whole_rows, gains[0])
     pieces = (
         lax.all_gather(query_weight, "fs", axis=0, tiled=True),
-        lax.all_gather(key_weight, "fs", axis=0, tiled=True),
+        keep_up_ranges(key_weight),
         lax.all_gather(value_weight, "fs", axis=0, tiled=True),
     )
     columns = scaled_one

time: 715 us -> 671 us (0.938)
  waiting for transfers between devices: 546 us -> 495 us
  starting transfers between devices: 0.39 us -> 7.63 us
    all_gather x1 -> x0, waiting for transfers between devices: 48.7 us -> none  [on_device(): lax.all_gather(key_weight, 'fs', axis=0, tiled=True)]
    all_to_all x0 -> x1, waiting for transfers between devices: none -> 32.4 us  [keep_up_ranges(): lax.all_to_all(jnp.stack([w_in for _ in range(lax.psum(1, 'fs'))], 0), 'f...]
    all_gather x1, waiting for transfers between devices: 44.7 us -> 16.7 us  [on_device(): lax.all_gather(query_weight, 'fs', axis=0, tiled=True)]
    all_to_all x0 -> x1, starting transfers between devices: none -> 7.28 us  [keep_up_ranges(): lax.all_to_all(jnp.stack([w_in for _ in range(lax.psum(1, 'fs'))], 0), 'f...]
  transfers between devices with their start and end apart: 11 -> 11, of which waited for: 10 -> 10; matrix products, arithmetic and copies ran while one was open for 16% -> 17% of each run, Pallas kernels for 0% -> 0%
where the time goes in v1:
time: 671 us; the launch traced here: 670 us
  waiting for transfers between devices  495 us (74%)
  matrix products  97.9 us (15%)
  local copies, waits for them, and re-layouts  30.8 us (5%)
  other arithmetic  19.3 us (3%)
  between operations  13.8 us (2%)
  starting transfers between devices  7.63 us (1%)
    all_gather x1, waiting for transfers between devices, on_device(): lax.all_gather(down_weight, 'fs', axis=1, tiled=True)  93.4 us
    all_gather x1, waiting for transfers between devices, on_device(): lax.all_gather(gate_up_weight, 'fs', axis=0, tiled=True)  91.8 us
    all_gather x1, waiting for transfers between devices, on_device(): lax.all_gather(value_up_weight, 'fs', axis=0, tiled=True)  83.5 us
    all_gather x1, waiting for transfers between devices, on_device(): lax.all_gather(value_weight, 'fs', axis=0, tiled=True)  61 us
    reduce_scatter x1, waiting for transfers between devices, on_device(): lax.psum_scatter(mixed_terms.astype(jnp.bfloat16), 'tp', scatter_dimensio...  36.5 us
    reduce_scatter x1, waiting for transfers between devices, on_device(): lax.psum_scatter(channel_terms.astype(jnp.bfloat16), 'tp', scatter_dimens...  36.1 us
    all_to_all x1, waiting for transfers between devices, keep_up_ranges(): lax.all_to_all(jnp.stack([w_in for _ in range(lax.psum(1, 'fs'))], 0), 'f...  32.4 us
    all_gather x1, waiting for transfers between devices, on_device(): middle_whole = lax.all_gather(middle, 'tp', axis=1, tiled=True)  26.3 us
  transfers between devices with their start and end apart: 11, of which 10 were waited for; matrix products, arithmetic and copies ran while one was open for 17% of the time, Pallas kernels for 0%

profile of v1, /device:TPU:0, one launch (start us, length us, event | category | flops | bytes accessed | tf_op | source)
XLA Modules:
  0.0 669.8 jit_solution(15204010763144161698)
XLA Ops:
  6.5 0.7 all-gather.9.cloned.1.call-update
  8.8 2.5 stack.11
  11.2 7.3 %all-to-all-start = ((bf16[8,256,512]{2,1,0:T(8,128)(2,1)}), bf16[8,256,512]{2,1,0:T(8,128)(2,1)S(1)}, u32[]{:S(2)}, u32[]{:S(2)}) async-start(bf16[8,256,512]{2,1,0:T(8,128)(2,1)} %stack.11), calls=%async_computation | async-start | bytes 4194304 | tf_op jit(solution)/shard_map/all_to_all | solution.py:17
  19.2 5.3 all_gather.28
  24.7 2.3 fusion.56
  27.5 12.7 %all-gather.9.cloned.1.call-done = bf16[768,2048]{1,0:T(8,128)(2,1)} async-done(((bf16[768,512]{1,0:T(8,128)(2,1)}), bf16[768,2048]{1,0:T(8,128)(2,1)}) %all-gather.9.cloned.1.call-update) | async-done | bytes 3145744 | tf_op jit(solution)/shard_map/all_gather | solution.py:98
  40.2 2.6 fusion.31
  42.8 32.4 %all-to-all-done = bf16[8,256,512]{2,1,0:T(8,128)(2,1)S(1)} async-done(((bf16[8,256,512]{2,1,0:T(8,128)(2,1)}), bf16[8,256,512]{2,1,0:T(8,128)(2,1)S(1)}, u32[]{:S(2)}, u32[]{:S(2)}) %all-to-all-start) | async-done | bytes 2097184 | tf_op jit(solution)/shard_map/all_to_all | solution.py:17
  75.2 3.7 multiply_convert_fusion.7
  79.6 16.7 %all-gather.13.cloned.1.call-done = bf16[2048,512]{1,0:T(8,128)(2,1)} async-done(((bf16[256,512]{1,0:T(8,128)(2,1)}), bf16[2048,512]{1,0:T(8,128)(2,1)}) %all-gather.13.cloned.1.call-update) | async-done | bytes 2097168 | tf_op jit(solution)/shard_map/all_gather | solution.py:103
  96.3 4.4 multiply_convert_fusion.6
  100.7 1.3 fusion.62
  102.0 1.4 copy.42
  103.4 2.3 copy.43
  105.7 1.8 multiply_subtract_fusion
  107.6 1.3 fusion.48
  108.8 61.0 %all-gather.11.cloned.1.call-done = bf16[2048,1024]{1,0:T(8,128)(2,1)} async-done(((bf16[256,1024]{1,0:T(8,128)(2,1)}), bf16[2048,1024]{1,0:T(8,128)(2,1)}) %all-gather.11.cloned.1.call-update) | async-done | bytes 4194320 | tf_op jit(solution)/shard_map/all_gather | solution.py:105
  169.8 8.2 %fusion.45 = f32[768,1024]{1,0:T(8,128)} fusion(bf16[2048,1024]{1,0:T(8,128)(2,1)} %all-gather.11.cloned.1.call-done, bf16[768,2048]{1,0:T(8,128)(2,1)} %all-gather.9.cloned.1.call-done, f32[2048]{0:T(1024)S(1)} %bitcast.96, f32[768]{0:T(1024)S(1)} %add_rsqrt_fusion.1), kind=kOutput, calls=%fused_computation.54 | convolution fusion | flops 3228303360 | bytes 10497024 | tf_op jit(solution)/shard_map/dot_general | solution.py:109
  178.0 5.6 reshape.169
  183.6 4.1 copy.48
  187.7 42.7 %while.15 = (s32[]{:T(128)}, f32[2,256,512]{2,1,0:T(8,128)S(1)}, f32[6,2,128,512]{3,2,1,0:T(8,128)}, f32[2]{0:T(128)S(1)}, f32[6,2,128,256]{3,2,0,1:T(8,128)}, /...) while((s32[]{:T(128)}, f32[2,256,512]{2,1,0:T(8,128)S(1)}, ...), condition=%wide.region_2.3_spmd.clone.clone.clone, body=%wide.region_1.2_spmd.clone.clone.clone.sunk | while | flops 1108771328 | bytes 7169184 | solution.py:68
  187.7 1.3 convolution_multiply_fusion.3
  189.1 1.6 fusion.88
  190.8 1.6 fusion.89
  192.4 2.4 convolution_add_fusion.2
  194.9 1.4 convolution_multiply_fusion.3
  196.2 1.6 fusion.88
  198.0 1.5 fusion.89
  199.5 2.5 convolution_add_fusion.2
  202.0 1.4 convolution_multiply_fusion.3
  203.3 1.6 fusion.88
  205.0 1.5 fusion.89
  206.6 2.5 convolution_add_fusion.2
  209.1 1.4 convolution_multiply_fusion.3
  210.5 1.6 fusion.88
  212.2 1.6 fusion.89
  213.7 2.4 convolution_add_fusion.2
  216.2 1.4 convolution_multiply_fusion.3
  217.6 1.6 fusion.88
  219.3 1.6 fusion.89
  220.9 2.5 convolution_add_fusion.2
  223.3 1.4 convolution_multiply_fusion.3
  224.7 1.6 fusion.88
  226.4 1.5 fusion.89
  227.9 2.5 convolution_add_fusion.2
  230.4 2.4 bitcast_reduce_fusion
  234.1 1.1 mul.367
  235.2 2.5 copy.46
  237.9 1.1 sub.65
  238.9 2.5 copy.45
  241.4 2.4 copy.34
  243.8 2.4 copy.44
  246.3 9.3 %convolution_convert_fusion = bf16[768,2048]{1,0:T(8,128)(2,1)} fusion(bf16[1024,2048]{1,0:T(8,128)(2,1)} %all-gather.15.cloned.1.call-done, f32[768,1024]{1,0:T(8,128)S(1)} %bitcast.84, f32[768,1024]{1,0:T(8,128)} %bitcast.86, f32[768,1024]{1,0:T(8,128)} %bitcast.85), kind=kOutput, calls=%fused_computation.44 | convolution fusion | flops 3225157632 | bytes 16777216 | tf_op jit(solution)/shard_map/dot_general | solution.py:132
  255.6 36.5 %reduce-scatter.3.cloned.1.call-done = bf16[768,512]{1,0:T(8,128)(2,1)} async-done(((bf16[768,2048]{1,0:T(8,128)(2,1)}), bf16[768,512]{1,0:T(8,128)(2,1)}) %reduce-scatter.3.cloned.1.call-update) | async-done | bytes 786448 | tf_op jit(solution)/shard_map/reduce_scatter | solution.py:137
  292.1 2.2 add_convert_fusion.1
  296.7 26.3 %all-gather.17.cloned.1.call-done = bf16[768,2048]{1,0:T(8,128)(2,1)} async-done(((bf16[768,512]{1,0:T(8,128)(2,1)}), bf16[768,2048]{1,0:T(8,128)(2,1)}) %all-gather.17.cloned.1.call-update) | async-done | bytes 3145744 | tf_op jit(solution)/shard_map/all_gather | solution.py:141
  323.0 2.7 fusion.33
  325.7 91.8 %all-gather.19.cloned.1.call-done = bf16[2048,1408]{1,0:T(8,128)(2,1)} async-done(((bf16[256,1408]{1,0:T(8,128)(2,1)}), bf16[2048,1408]{1,0:T(8,128)(2,1)}) %all-gather.19.cloned.1.call-update) | async-done | bytes 5767184 | tf_op jit(solution)/shard_map/all_gather | solution.py:145
  417.5 9.2 %fusion.34 = f32[768,1408]{1,0:T(8,128)} fusion(bf16[2048,1408]{1,0:T(8,128)(2,1)} %all-gather.19.cloned.1.call-done, bf16[768,2048]{1,0:T(8,128)(2,1)S(1)} %copy-done.2, f32[2048]{0:T(1024)S(1)} %bitcast.92, f32[768]{0:T(1024)S(1)} %add_rsqrt_fusion), kind=kOutput, calls=%fused_computation.45 | convolution fusion | flops 4437147648 | bytes 13249536 | tf_op jit(solution)/shard_map/dot_general | solution.py:149
  426.7 83.5 %all-gather.21.cloned.1.call-done = bf16[2048,1408]{1,0:T(8,128)(2,1)} async-done(((bf16[256,1408]{1,0:T(8,128)(2,1)}), bf16[2048,1408]{1,0:T(8,128)(2,1)}) %all-gather.21.cloned.1.call-update) | async-done | bytes 5767184 | tf_op jit(solution)/shard_map/all_gather | solution.py:144
  510.2 93.4 %all-gather.23.cloned.1.call-done = bf16[1408,2048]{1,0:T(8,128)(2,1)} async-done(((bf16[1408,256]{1,0:T(8,128)(2,1)}), bf16[1408,2048]{1,0:T(8,128)(2,1)}) %all-gather.23.cloned.1.call-update) | async-done | bytes 5767184 | tf_op jit(solution)/shard_map/all_gather | solution.py:161
  603.6 21.1 %convolution_convert_fusion.1 = bf16[768,2048]{1,0:T(8,128)(2,1)} fusion(bf16[1408,2048]{1,0:T(8,128)(2,1)} %all-gather.23.cloned.1.call-done, f32[768,1408]{1,0:T(8,128)} %fusion.34, bf16[2048,1408]{1,0:T(8,128)(2,1)} %all-gather.21.cloned.1.call-done, bf16[768,2048]{1,0:T(8,128)(2,1)S(1)} %copy-done.2, f32[2048]{0:T(1024)S(1)} %bitcast.93, ...), kind=kOutput, calls=%fused_computation.46 | convolution fusion | flops 8880881664 | bytes 22184960 | tf_op jit(solution)/shard_map/dot_general | solution.py:159
  624.7 36.1 %reduce-scatter.5.cloned.1.call-done = bf16[768,512]{1,0:T(8,128)(2,1)} async-done(((bf16[768,2048]{1,0:T(8,128)(2,1)}), bf16[768,512]{1,0:T(8,128)(2,1)}) %reduce-scatter.5.cloned.1.call-update) | async-done | bytes 786448 | tf_op jit(solution)/shard_map/reduce_scatter | solution.py:164
  660.8 2.2 add_convert_fusion
  (72 shorter events, 7.9 us)
Async XLA Ops:
  6.5 33.7 %all-gather.9.cloned.1.call-start = ((), (), s32[]{:S(2)}) async-start(), calls=%async_computation.3 | async-start | bytes 3932160 | tf_op jit(solution)/shard_map/all_gather | solution.py:98
  7.3 89.0 %all-gather.13.cloned.1.call-start = ((), (), s32[]{:S(2)}) async-start(), calls=%async_computation.5 | async-start | bytes 2359296 | tf_op jit(solution)/shard_map/all_gather | solution.py:103
  8.0 161.8 %all-gather.11.cloned.1.call-start = ((), (), s32[]{:S(2)}) async-start(), calls=%async_computation.4 | async-start | bytes 4718592 | tf_op jit(solution)/shard_map/all_gather | solution.py:105
  8.7 10.4 %copy-start.9 = (bf16[512]{0:T(512)(128)(2,1)S(1)}, bf16[512]{0:T(512)(128)(2,1)}, u32[]{:S(2)}) copy-start(bf16[512]{0:T(512)(128)(2,1)} %param.16) | copy-start | bytes 3076
  8.8 10.4 %copy-start.10 = (bf16[512]{0:T(512)(128)(2,1)S(1)}, bf16[512]{0:T(512)(128)(2,1)}, u32[]{:S(2)}) copy-start(bf16[512]{0:T(512)(128)(2,1)} %param.22) | copy-start | bytes 3076
  8.8 15.9 %copy-start.5 = (f32[2]{0:T(128)S(1)}, f32[2]{0:T(128)}, u32[]{:S(2)}) copy-start(f32[2]{0:T(128)} %param.20) | copy-start | bytes 28
  11.2 63.9 %all-to-all-start = ((bf16[8,256,512]{2,1,0:T(8,128)(2,1)}), bf16[8,256,512]{2,1,0:T(8,128)(2,1)S(1)}, u32[]{:S(2)}, u32[]{:S(2)}) async-start(bf16[8,256,512]{2,1,0:T(8,128)(2,1)} %stack.11), calls=%async_computation | async-start | bytes 4194304 | tf_op jit(solution)/shard_map/all_to_all | solution.py:17
  18.5 227.7 %all-gather.15.cloned.1.call-start = ((), (), s32[]{:S(2)}) async-start(), calls=%async_computation.6 | async-start | bytes 4718592 | tf_op jit(solution)/shard_map/all_gather | solution.py:134
  19.1 273.0 %reduce-scatter.3.cloned.1.call-start = ((), (), s32[]{:S(2)}) async-start(), calls=%async_computation.7 | async-start | bytes 3932160 | tf_op jit(solution)/shard_map/reduce_scatter | solution.py:137
  230.4 2.9 copy-start
  243.8 2.4 copy-start.3
  255.5 36.6 %copy-start.4 = (bf16[768,512]{1,0:T(8,128)(2,1)S(1)}, bf16[768,512]{1,0:T(8,128)(2,1)}, u32[]{:S(2)}) copy-start(bf16[768,512]{1,0:T(8,128)(2,1)} %param.15) | copy-start | bytes 2359300
  255.6 41.1 %copy-start.8 = (bf16[1408]{0:T(1024)(128)(2,1)S(1)}, bf16[1408]{0:T(1024)(128)(2,1)}, u32[]{:S(2)}) copy-start(bf16[1408]{0:T(1024)(128)(2,1)} %param.26) | copy-start | bytes 8452
  255.6 41.1 %copy-start.6 = (bf16[3,1408]{1,0:T(4,128)(2,1)S(1)}, bf16[3,1408]{1,0:T(4,128)(2,1)}, u32[]{:S(2)}) copy-start(bf16[3,1408]{1,0:T(4,128)(2,1)} %param.25) | copy-start | bytes 25348
  255.6 67.4 %all-gather.17.cloned.1.call-start = ((), (), s32[]{:S(2)}) async-start(), calls=%async_computation.8 | async-start | bytes 3932160 | tf_op jit(solution)/shard_map/all_gather | solution.py:141
  294.3 123.2 %copy-start.7 = (f32[1,2048]{1,0:T(1,128)S(1)}, f32[1,2048]{1,0:T(1,128)}, u32[]{:S(2)}) copy-start(f32[1,2048]{1,0:T(1,128)} %get-tuple-element.238) | copy-start | bytes 24580
  294.3 123.2 %all-gather.19.cloned.1.call-start = ((), (), s32[]{:S(2)}) async-start(), calls=%async_computation.9 | async-start | bytes 6488064 | tf_op jit(solution)/shard_map/all_gather | solution.py:145
  295.1 215.1 %all-gather.21.cloned.1.call-start = ((), (), s32[]{:S(2)}) async-start(), calls=%async_computation.10 | async-start | bytes 6488064 | tf_op jit(solution)/shard_map/all_gather | solution.py:144
  295.8 307.8 %all-gather.23.cloned.1.call-start = ((), (), s32[]{:S(2)}) async-start(), calls=%async_computation.11 | async-start | bytes 6488064 | tf_op jit(solution)/shard_map/all_gather | solution.py:161
  296.6 364.2 %reduce-scatter.5.cloned.1.call-start = ((), (), s32[]{:S(2)}) async-start(), calls=%async_computation.12 | async-start | bytes 3932160 | tf_op jit(solution)/shard_map/reduce_scatter | solution.py:164
  323.0 94.5 %copy-start.2 = (bf16[768,2048]{1,0:T(8,128)(2,1)S(1)}, bf16[768,2048]{1,0:T(8,128)(2,1)}, u32[]{:S(2)}) copy-start(bf16[768,2048]{1,0:T(8,128)(2,1)} %all-gather.17.cloned.1.call-done) | copy-start | bytes 9437188
  624.7 36.1 %copy-start.1 = (bf16[768,512]{1,0:T(8,128)(2,1)S(1)}, bf16[768,512]{1,0:T(8,128)(2,1)}, u32[]{:S(2)}) copy-start(bf16[768,512]{1,0:T(8,128)(2,1)} %add_convert_fusion.1) | copy-start | bytes 2359300
Sparse Core Ops, SparseCore 0:
  8.9 31.2 all-gather.8
  42.3 53.9 all-gather.12
  98.4 71.3 all-gather.10
  171.7 73.1 all-gather.14
  255.7 36.3 reduce-scatter.2
  294.5 28.4 all-gather.16
  325.2 92.2 all-gather.18
  419.7 90.4 all-gather.20
  512.3 91.2 all-gather.22
  624.8 35.8 reduce-scatter.4
